TPU v7x, 512 devices: a whole 4x4x16 slice. The times are simulated.
512 devices in a mesh: sp: 64 (over z, y), dp: 8 (over x, core).
Axes of the slice: x: 4, y: 4, z: 16, core: 2. Of those that a mesh axis runs over, the one named last changes fastest.
Arguments:
- tokens: bfloat16 [16384, 2048], P('sp'), may hold values from -16 to 16
- w_carry: bfloat16 [2048, 1024], P(None, 'dp'), may hold values from -0.125 to 0.125
- w_gate: bfloat16 [2048, 1024], P(None, 'dp'), may hold values from -8 to 8
- mix_weight: bfloat16 [8, 128, 128], P('dp'), may hold values from -0.5 to 0.5
- mix_bias: float32 [8, 128], P('dp'), may hold values from 0.1 to 1.9
- ln_gain: float32 [1024], P('dp'), may hold values from 0.1 to 1.9
- ln_shift: float32 [1024], P('dp'), may hold values from -3 to 3
- cotangent: bfloat16 [16384, 1024], P('sp', 'dp'), may hold values from -6 to 6
Outputs:
- grad_input: bfloat16 [16384, 2048], P('sp')
- grad_carry: float32 [2048, 1024], P('sp', 'dp')
- grad_gate: float32 [2048, 1024], P('sp', 'dp')
- grad_mix: float32 [8, 128, 128], P('dp')
- grad_bias: float32 [8, 128], P('dp')
- grad_gain: float32 [1024], P('dp')
- grad_shift: float32 [1024], P('dp')
All inputs are finite; a program needn't handle non-finite values.
Results may differ from a plain program's by a relative error of at most 0.017.
Values may be sent and summed in bfloat16 or wider, within the bound.
No kernel may reach another device: no remote copies, remote signals or barrier semaphores. Data moves between devices by JAX's collectives and lax.ppermute only.
A program may use at most 64 MiB of HBM per device.

v0:
```python
import math

import jax
import jax.numpy as jnp
from jax import lax
from jax.sharding import Mesh
from jax.sharding import PartitionSpec as P

GROUP_DIM = 128
SPAN = 128
SEGMENT = 64
SP = ("sp_0", "sp_1")


sqrt_half = 0.7071067811865476
density = 0.3989422804014327
epsilon = 1e-06


def sent_to_all(value, axis):
    copies = jnp.broadcast_to(value, (lax.axis_size(axis), *value.shape))
    return lax.all_to_all(copies, axis, split_axis=0, concat_axis=0, tiled=True)


def of_everyone(value, axis):
    return sent_to_all(value, axis).sum(axis=0)


def together(arrays, axis):
    ends = [0]
    for a in arrays:
        ends.append(ends[-1] + a.size)
    total = of_everyone(jnp.concatenate([a.ravel() for a in arrays]), axis)
    return tuple((total[b:e].reshape(a.shape) for a, b, e in zip(arrays, ends, ends[1:])))


def gathered_total(value, axis):
    tiles = lax.all_gather(value, axis).astype(jnp.float32)
    return tiles.sum(axis=0)


def sum_in_order(tiles, axes, sequence):
    inside = tiles.shape[1:]
    tiles = tiles.reshape(*(lax.axis_size(a) for a in axes), *inside)
    tiles = jnp.moveaxis(tiles, sequence, range(len(axes))).reshape(-1, *inside)
    for k in sequence:
        tiles = lax.psum_scatter(tiles, axes[k], scatter_dimension=0, tiled=True)
    return tiles[0]


def cut_along(value, dim, length):
    shape = value.shape
    tiles = value.reshape(*shape[:dim], length, shape[dim] // length, *shape[dim + 1 :])
    return jnp.moveaxis(tiles, dim, 0)


def sum_by_axis(value, axes, sequence, dim):
    length = lax.axis_size(axes)
    return sum_in_order(cut_along(value, dim, length), axes, sequence)


def filled_up(lines, length):
    spare = -len(lines) % length
    return jnp.pad(lines, [(0, spare)] + [(0, 0)] * (lines.ndim - 1))


def in_order(tiles, dim):
    shape = list(tiles.shape[1:])
    shape[dim] *= tiles.shape[0]
    return jnp.moveaxis(tiles, 0, dim).reshape(shape)


def collect(value, axis, dim):
    tiles = sent_to_all(value, axis)
    return in_order(tiles, dim)


def sent_and_summed(value, axis, dim):
    tiles = cut_along(value, dim, lax.axis_size(axis))
    arrived = lax.all_to_all(tiles, axis, split_axis=0, concat_axis=0, tiled=True)
    return arrived.sum(axis=0)


def sum_by_parts(value, axes):
    padded = filled_up(value, lax.axis_size(axes))
    whole = collect(sent_and_summed(padded, axes, 0), axes, 0)
    return lax.slice_in_dim(whole, 0, len(value)).reshape(value.shape)


def together_2(arrays, axis):
    vector, at, finished = (jnp.concatenate([a.reshape(-1) for a in arrays]), 0, [])
    total = sum_by_parts(vector, axis)
    for a in arrays:
        finished.append(total[at : at + a.size].reshape(a.shape))
        at += a.size
    return tuple(finished)


def gelu_slope(inputs):
    return (
        0.5 * (1.0 + lax.erf(inputs * sqrt_half))
        + inputs * jnp.exp(-0.5 * inputs * inputs) * density
    )


def block_visible():
    segment = jnp.arange(SPAN) // SEGMENT
    return (segment[:, None] >= segment[None, :]).astype(jnp.float32)


def grad_term(tokens, grad_rows):
    return jnp.einsum("tr,tc->rc", tokens, grad_rows, preferred_element_type=jnp.float32)


def shards(tokens, w_carry, w_gate, mix_weight, mix_bias, ln_gain, ln_shift, cotangent):
    highest = lax.Precision.HIGHEST
    owned = w_carry.shape[1]
    channels = owned * lax.axis_size("dp")
    groups = mix_weight.shape[0]
    blocks = tokens.shape[0] // SPAN
    loss_scale = 1.0 / math.sqrt(tokens.shape[0] * lax.axis_size(SP))
    carry_pre = jnp.dot(tokens, w_carry, preferred_element_type=jnp.float32).astype(jnp.bfloat16)
    gate_pre = jnp.dot(tokens, w_gate, preferred_element_type=jnp.float32).astype(jnp.bfloat16)
    carry_wide = carry_pre.astype(jnp.float32)
    gate_wide = gate_pre.astype(jnp.float32)
    carried = jax.nn.gelu(carry_wide, approximate=False)
    gate_act = jax.nn.gelu(gate_wide, approximate=False)
    moment_one, second = together(
        (jnp.sum(gate_act, axis=1), jnp.sum(gate_act * gate_act, axis=1)), "dp"
    )
    average = moment_one[:, None] / channels
    centered = gate_act - average
    variance = second[:, None] / channels - average * average
    rstd = lax.rsqrt(variance + epsilon)
    normed = centered * rstd
    gated_in = normed * ln_gain[None, :] + ln_shift[None, :]
    weights = mix_weight.astype(jnp.float32) * block_visible()[None]
    gated_four = gated_in.reshape(blocks, SPAN, groups, GROUP_DIM)
    spatial = jnp.einsum("gts,nsgc->ntgc", weights, gated_four, precision=highest)
    spatial = (spatial + mix_bias.T[None, :, :, None]).reshape(tokens.shape[0], owned)
    upstream = cotangent.astype(jnp.float32)
    d_carry_pre = (upstream * spatial * gelu_slope(carry_wide)).astype(jnp.bfloat16)
    d_spatial = (upstream * carried).reshape(blocks, SPAN, groups, GROUP_DIM)
    d_gated_four = jnp.einsum("gts,ntgc->nsgc", weights, d_spatial, precision=highest)
    d_gated_in = d_gated_four.reshape(tokens.shape[0], owned)
    d_normed = d_gated_in * ln_gain[None, :]
    sum_plain, sum_cross = together(
        (jnp.sum(d_normed, axis=1), jnp.sum(d_normed * normed, axis=1)), "dp"
    )
    d_gate_act = rstd * (
        d_normed - sum_plain[:, None] / channels - normed * (sum_cross[:, None] / channels)
    )
    d_gate_pre = (d_gate_act * gelu_slope(gate_wide)).astype(jnp.bfloat16)
    partial_value = jnp.einsum(
        "tc,dc->td", d_carry_pre, w_carry, preferred_element_type=jnp.float32
    )
    partial_value = partial_value + jnp.einsum(
        "tc,dc->td", d_gate_pre, w_gate, preferred_element_type=jnp.float32
    )
    grad_input = (
        gathered_total(partial_value.astype(jnp.bfloat16), "dp")
        .astype(jnp.float32)
        .astype(jnp.bfloat16)
    )
    both_grads = jnp.concatenate([d_carry_pre, d_gate_pre], axis=1)
    summed = (
        sum_by_axis(grad_term(tokens, both_grads).astype(jnp.bfloat16), SP, (1, 0), 0).astype(
            jnp.float32
        )
        * loss_scale
    )
    grad_carry = summed[:, :owned]
    grad_gate = summed[:, owned:]
    mix_term = (
        jnp.einsum("ntgc,nsgc->gts", d_spatial, gated_four, precision=highest)
        * block_visible()[None]
    )
    bias_term = jnp.sum(d_spatial, axis=(0, 3)).T
    gain_term = jnp.sum(d_gated_in * normed, axis=0)
    shift_term = jnp.sum(d_gated_in, axis=0)
    grad_mix, grad_bias, grad_gain, grad_shift = together_2(
        (mix_term, bias_term, gain_term, shift_term), SP
    )
    return (
        grad_input,
        grad_carry,
        grad_gate,
        grad_mix * loss_scale,
        grad_bias * loss_scale,
        grad_gain * loss_scale,
        grad_shift * loss_scale,
    )


def solution(mesh):
    finer = Mesh(mesh.devices.reshape(16, 4, mesh.shape["dp"]), ("sp_0", "sp_1", "dp"))
    placed = (
        P(SP, None),
        P(None, "dp"),
        P(None, "dp"),
        P("dp", None, None),
        P("dp", None),
        P("dp"),
        P("dp"),
        P(SP, "dp"),
    )
    return jax.shard_map(
        shards,
        mesh=finer,
        in_specs=placed,
        out_specs=(
            P(SP, None),
            P(SP, "dp"),
            P(SP, "dp"),
            P("dp", None, None),
            P("dp", None),
            P("dp"),
            P("dp"),
        ),
        check_vma=False,
    )
```

profile of v0, /device:TPU:8, one launch (start us, length us, event | category | flops | bytes accessed | tf_op | source)
XLA Modules:
  0.0 155.7 jit_solution(3094841536010879101)
XLA Ops:
  8.0 0.0 copy-start
  8.0 0.0 copy-start.7
  8.1 0.0 copy-start.4
  8.1 1.2 copy-done
  9.2 1.9 %fusion.58 = (f32[256]{0:T(256)S(1)}, f32[256]{0:T(256)S(1)}, f32[256,128]{1,0:T(8,128)S(1)}, f32[256,128]{1,0:T(8,128)S(1)}) fusion(bf16[256,2048]{1,0:T(8,128)(2,1)S(1)} %copy-done, bf16[2048,128]{1,0:T(8,128)(2,1)} %param.10), kind=kOutput, calls=%fused_computation.111 | convolution fusion | flops 136478208 | bytes 1837056 | tf_op jit(solution)/shard_map/dot_general | solution.py:123
  11.1 0.6 broadcast_in_dim.6
  11.7 4.3 %all-to-all-start = ((f32[8,1,512]{2,1,0:T(1,128)}), f32[8,1,512]{2,1,0:T(1,128)S(1)}, u32[]{:S(2)}, u32[]{:S(2)}) async-start(f32[8,1,512]{2,1,0:T(1,128)} %broadcast_in_dim.6), calls=%async_computation | async-start | bytes 32768 | tf_op jit(solution)/shard_map/all_to_all | solution.py:22
  16.0 0.0 reduce-scatter.3.cloned.1.call-start
  16.1 5.3 %all-to-all-done = f32[8,1,512]{2,1,0:T(1,128)S(1)} async-done(((f32[8,1,512]{2,1,0:T(1,128)}), f32[8,1,512]{2,1,0:T(1,128)S(1)}, u32[]{:S(2)}, u32[]{:S(2)}) %all-to-all-start) | async-done | bytes 16416 | tf_op jit(solution)/shard_map/all_to_all | solution.py:22
  21.5 0.1 multiply_add_fusion
  21.6 0.0 copy-done.6
  21.6 0.0 copy-done.9
  21.6 0.3 fusion.2
  21.9 0.8 fusion.59
  22.8 0.5 fusion.27
  23.2 0.2 fusion.26
  23.5 7.7 %all_to_all.27 = f32[8,1,512]{2,1,0:T(1,128)S(1)} all-to-all(f32[8,1,512]{2,1,0:T(1,128)S(1)} %broadcast_in_dim.7), channel_id=1, replica_groups=mesh['sp_0'=16,'sp_1'=4,'dp'=8] {'dp'}, dimensions={0} | all-to-all | bytes 32768 | tf_op jit(solution)/shard_map/all_to_all | solution.py:22
  31.2 0.2 fusion.22
  31.5 0.5 fusion.1
  31.9 0.5 copy.31
  32.5 0.0 copy-start.5
  32.5 1.1 copy.32
  33.5 0.0 reduce-scatter.3.cloned.1.call-update
  33.6 0.0 reduce-scatter.5.cloned.1.call-start
  33.6 31.7 %reduce-scatter.3.cloned.1.call-done = bf16[16,32,256]{2,1,0:T(8,128)(2,1)} async-done(((bf16[64,32,256]{2,1,0:T(8,128)(2,1)}), bf16[16,32,256]{2,1,0:T(8,128)(2,1)}) %reduce-scatter.3.cloned.1.call-update) | async-done | bytes 262160 | tf_op jit(solution)/shard_map/reduce_scatter | solution.py:47
  65.3 0.0 reduce-scatter.5.cloned.1.call-update
  65.3 0.0 all-gather.3.cloned.1.call-start
  65.4 0.4 fusion.62
  65.8 0.0 copy-done.1
  65.8 0.0 copy-start.3
  65.9 1.4 fusion
  67.3 0.0 all-gather.3.cloned.1.call-update
  67.3 0.1 reduce_sum.123
  67.4 0.3 fusion.6
  67.7 0.3 all_to_all.20
  67.9 31.2 %all_to_all.28 = f32[64,1,262]{2,1,0:T(1,128)S(1)} all-to-all(f32[64,1,262]{2,1,0:T(1,128)S(1)} %all_to_all.20), channel_id=1, replica_groups=mesh['sp_0'=16,'sp_1'=4,'dp'=8] {'sp_0','sp_1'}, dimensions={0} | all-to-all | bytes 134144 | tf_op jit(solution)/shard_map/all_to_all | solution.py:80
  99.2 0.1 reduce_sum.124
  99.3 0.1 broadcast_in_dim.8
  99.3 19.4 %all_to_all.29 = f32[64,1,262]{2,1,0:T(1,128)S(1)} all-to-all(f32[64,1,262]{2,1,0:T(1,128)S(1)} %broadcast_in_dim.8), channel_id=1, replica_groups=mesh['sp_0'=16,'sp_1'=4,'dp'=8] {'sp_0','sp_1'}, dimensions={0} | all-to-all | bytes 134144 | tf_op jit(solution)/shard_map/all_to_all | solution.py:22
  118.8 0.2 reduce.11
  119.0 0.2 reshape.180
  119.2 0.2 slice.39
  119.4 0.5 slice_multiply_fusion.4
  120.0 0.6 fusion.42
  120.6 19.9 %reduce-scatter.5.cloned.1.call-done = bf16[1,32,256]{2,1,0:T(8,128)(2,1)} async-done(((bf16[16,32,256]{2,1,0:T(8,128)(2,1)}), bf16[1,32,256]{2,1,0:T(8,128)(2,1)}) %reduce-scatter.5.cloned.1.call-update) | async-done | bytes 16400 | tf_op jit(solution)/shard_map/reduce_scatter | solution.py:47
  140.5 0.7 multiply_bitcast_fusion
  141.3 0.6 fusion.61
  141.9 6.4 %reduce_sum.118 = bf16[256,2048]{1,0:T(8,128)(2,1)} reduce(bf16[8,256,2048]{2,1,0:T(8,128)(2,1)} %bitcast.74, bf16[]{:T(256)} %constant.103.clone.1), dimensions={0}, to_apply=%region_6.7 | reduce | flops 3670016 | bytes 9437186 | tf_op jit(solution)/shard_map/reduce_sum | solution.py:39
  (24 shorter events, 0.2 us)
Async XLA Ops:
  8.0 1.2 copy-start
  8.0 13.4 %copy-start.7 = (f32[128]{0:T(128)S(1)}, f32[128]{0:T(128)}, u32[]{:S(2)}) copy-start(f32[128]{0:T(128)} %param.13) | copy-start | bytes 1540
  8.0 13.4 %copy-start.8 = (f32[128]{0:T(128)S(1)}, f32[128]{0:T(128)}, u32[]{:S(2)}) copy-start(f32[128]{0:T(128)} %param.14) | copy-start | bytes 1540
  8.0 13.6 %copy-start.6 = (bf16[1,128,128]{2,1,0:T(8,128)(2,1)S(1)}, bf16[1,128,128]{2,1,0:T(8,128)(2,1)}, u32[]{:S(2)}) copy-start(bf16[1,128,128]{2,1,0:T(8,128)(2,1)} %param.11) | copy-start | bytes 98308
  8.0 13.6 %copy-start.9 = (f32[1,128]{1,0:T(1,128)S(1)}, f32[1,128]{1,0:T(1,128)}, u32[]{:S(2)}) copy-start(f32[1,128]{1,0:T(1,128)} %param.12) | copy-start | bytes 1540
  8.1 13.9 %copy-start.4 = (bf16[2048,128]{1,0:T(8,128)(2,1)S(1)}, bf16[2048,128]{1,0:T(8,128)(2,1)}, u32[]{:S(2)}) copy-start(bf16[2048,128]{1,0:T(8,128)(2,1)} %param.9) | copy-start | bytes 1572868
  9.2 12.7 %copy-start.10 = (bf16[256,128]{1,0:T(8,128)(2,1)S(1)}, bf16[256,128]{1,0:T(8,128)(2,1)}, u32[]{:S(2)}) copy-start(bf16[256,128]{1,0:T(8,128)(2,1)} %param.15) | copy-start | bytes 196612
  11.7 9.7 %all-to-all-start = ((f32[8,1,512]{2,1,0:T(1,128)}), f32[8,1,512]{2,1,0:T(1,128)S(1)}, u32[]{:S(2)}, u32[]{:S(2)}) async-start(f32[8,1,512]{2,1,0:T(1,128)} %broadcast_in_dim.6), calls=%async_computation | async-start | bytes 32768 | tf_op jit(solution)/shard_map/all_to_all | solution.py:22
  16.0 49.3 %reduce-scatter.3.cloned.1.call-start = ((), (), s32[]{:S(2)}) async-start(), calls=%async_computation.6 | async-start | bytes 1310720 | tf_op jit(solution)/shard_map/reduce_scatter | solution.py:47
  22.8 8.7 %copy-start.2 = (f32[256,128]{1,0:T(8,128)}, f32[256,128]{1,0:T(8,128)S(1)}, u32[]{:S(2)}) copy-start(f32[256,128]{1,0:T(8,128)S(1)} %get-tuple-element.12) | copy-start | bytes 393220
  32.5 32.9 %copy-start.5 = (bf16[2048,128]{1,0:T(8,128)(2,1)S(1)}, bf16[2048,128]{1,0:T(8,128)(2,1)}, u32[]{:S(2)}) copy-start(bf16[2048,128]{1,0:T(8,128)(2,1)} %param.9) | copy-start | bytes 1572868
  33.5 32.3 %copy-start.1 = (bf16[2048,128]{1,0:T(8,128)(2,1)S(1)}, bf16[2048,128]{1,0:T(8,128)(2,1)}, u32[]{:S(2)}) copy-start(bf16[2048,128]{1,0:T(8,128)(2,1)} %param.10) | copy-start | bytes 1572868
  33.6 107.0 %reduce-scatter.5.cloned.1.call-start = ((), (), s32[]{:S(2)}) async-start(), calls=%async_computation.7 | async-start | bytes 278528 | tf_op jit(solution)/shard_map/reduce_scatter | solution.py:47
  65.3 76.5 %all-gather.3.cloned.1.call-start = ((), (), s32[]{:S(2)}) async-start(), calls=%async_computation.8 | async-start | bytes 9437184 | tf_op jit(solution)/shard_map/all_gather | solution.py:38
  65.8 1.5 copy-start.3
Sparse Core Ops, SparseCore 0:
  33.7 31.5 reduce-scatter.2
  68.1 72.3 reduce-scatter.4
Sparse Core Ops, SparseCore 1:
  68.5 59.3 all-gather.2
where the time goes:
time: 156 us
  blocking collectives  58.4 us (37%)
  waiting for transfers between devices  57 us (37%)
  between operations  15.7 us (10%)
  other arithmetic  9.34 us (6%)
  matrix products  6.03 us (4%)
  local copies, waits for them, and re-layouts  4.76 us (3%)
  starting transfers between devices  4.42 us (3%)
    reduce_scatter x2, waiting for transfers between devices, sum_in_order(): tiles = lax.psum_scatter(tiles, axes[k], scatter_dimension=0, tiled=True)  51.6 us
    all_to_all x1, blocking collectives, sent_and_summed(): lax.all_to_all(tiles, axis, split_axis=0, concat_axis=0, tiled=True)  31.2 us
    all_to_all x2, blocking collectives, sent_to_all(): return lax.all_to_all(copies, axis, split_axis=0, concat_axis=0, tiled=True)  27.2 us
    reduce_sum x1, other arithmetic, gathered_total(): return tiles.sum(axis=0)  6.39 us
    all_to_all x1, waiting for transfers between devices, sent_to_all(): return lax.all_to_all(copies, axis, split_axis=0, concat_axis=0, tiled=True)  5.3 us
    all_to_all x1, starting transfers between devices, sent_to_all(): return lax.all_to_all(copies, axis, split_axis=0, concat_axis=0, tiled=True)  4.3 us
  transfers between devices with their start and end apart: 4, of which 3 were waited for; matrix products, arithmetic and copies ran while one was open for 4% of the time, Pallas kernels for 0%

commit v1 on v0

v1 whole, which is shorter than its diff:
```python
import math

import jax
import jax.numpy as jnp
from jax import lax
from jax.sharding import Mesh
from jax.sharding import PartitionSpec as P

GROUP_DIM = 128
SPAN = 128
SEGMENT = 64
SP = ("z", "y")
DP = ("x", "c")
SWAP = ((0, 1), (1, 0))

sqrt_half = 0.7071067811865476
density = 0.3989422804014327
epsilon = 1e-06
bf16 = jnp.bfloat16
f32 = jnp.float32


def exchange(tiles, axes):
    return lax.all_to_all(tiles, axes, split_axis=0, concat_axis=0, tiled=True)


def to_all(value, axes):
    return exchange(jnp.broadcast_to(value, (lax.axis_size(axes), *value.shape)), axes)


def gelu_slope(inputs):
    return (
        0.5 * (1.0 + lax.erf(inputs * sqrt_half))
        + inputs * jnp.exp(-0.5 * inputs * inputs) * density
    )


def block_visible():
    segment = jnp.arange(SPAN) // SEGMENT
    return (segment[:, None] >= segment[None, :]).astype(f32)


def two_parts(value):
    high = lax.reduce_precision(value, 8, 7)
    return high.astype(bf16), (value - high).astype(bf16)


def shards(tokens, w_carry, w_gate, mix_weight, mix_bias, ln_gain, ln_shift, cotangent):
    highest = lax.Precision.HIGHEST
    rows, model = tokens.shape
    owned = w_carry.shape[1]
    n_dp = lax.axis_size(DP)
    n_x, n_y, n_z = lax.axis_size("x"), lax.axis_size("y"), lax.axis_size("z")
    channels = owned * n_dp
    blocks = rows // SPAN
    loss_scale = 1.0 / math.sqrt(rows * n_y * n_z)

    carry_pre = jnp.dot(tokens, w_carry, preferred_element_type=f32).astype(bf16)
    gate_pre = jnp.dot(tokens, w_gate, preferred_element_type=f32).astype(bf16)
    carry_wide = carry_pre.astype(f32)
    gate_wide = gate_pre.astype(f32)
    carried = jax.nn.gelu(carry_wide, approximate=False)
    gate_act = jax.nn.gelu(gate_wide, approximate=False)
    upstream = cotangent.astype(f32)
    weights = mix_weight[0].astype(f32) * block_visible()
    d_spatial = upstream * carried
    d_spatial_b = d_spatial.reshape(blocks, SPAN, owned)
    d_gated_in = jnp.einsum("ts,ntc->nsc", weights, d_spatial_b, precision=highest)
    d_gated_in = d_gated_in.reshape(rows, owned)
    d_normed = d_gated_in * ln_gain[None, :]

    mean_a = jnp.mean(gate_act, axis=1)
    mean_d = jnp.mean(d_normed, axis=1)
    off_a = gate_act - mean_a[:, None]
    square = jnp.sum(off_a * off_a, axis=1)
    cross = jnp.sum(off_a * (d_normed - mean_d[:, None]), axis=1)
    stats = jnp.stack([mean_a, mean_d, square, cross]).reshape(4 * blocks, SPAN)
    stats = to_all(stats, DP).reshape(n_dp, 4, rows)
    average = jnp.mean(stats[:, 0], axis=0)
    d_average = jnp.mean(stats[:, 1], axis=0)
    shift_a = stats[:, 0] - average
    shift_d = stats[:, 1] - d_average
    square = jnp.sum(stats[:, 2], axis=0) + owned * jnp.sum(shift_a * shift_a, axis=0)
    cross = jnp.sum(stats[:, 3], axis=0) + owned * jnp.sum(shift_a * shift_d, axis=0)
    rstd = lax.rsqrt(square / channels + epsilon)
    slope_in = rstd * cross / channels

    normed = (gate_act - average[:, None]) * rstd[:, None]
    gated_in = normed * ln_gain[None, :] + ln_shift[None, :]
    gated_b = gated_in.reshape(blocks, SPAN, owned)
    spatial = jnp.einsum("ts,nsc->ntc", weights, gated_b, precision=highest)
    spatial = (spatial + mix_bias[0][None, :, None]).reshape(rows, owned)
    d_carry_pre = (upstream * spatial * gelu_slope(carry_wide)).astype(bf16)
    d_gate_act = rstd[:, None] * (
        d_normed - d_average[:, None] - normed * slope_in[:, None]
    )
    d_gate_pre = (d_gate_act * gelu_slope(gate_wide)).astype(bf16)
    d_pre = jnp.concatenate([d_carry_pre, d_gate_pre], axis=1)

    mix_term = jnp.einsum("ntc,nsc->ts", d_spatial_b, gated_b, precision=highest)
    bias_term = jnp.sum(d_spatial_b, axis=(0, 2))
    gain_term = jnp.sum(d_gated_in * normed, axis=0)
    shift_term = jnp.sum(d_gated_in, axis=0)
    corner = mix_term[:SEGMENT, :SEGMENT]
    seen = jnp.concatenate(
        [
            mix_term[SEGMENT:],
            jnp.concatenate([corner[: SEGMENT // 2], corner[SEGMENT // 2 :]], axis=1),
        ]
    )
    part = seen.shape[0] // n_y
    lines = jnp.stack([bias_term, gain_term, shift_term, jnp.zeros_like(bias_term)])
    small = jnp.concatenate(
        [seen.reshape(n_y, part, SPAN), lines[:, None], jnp.zeros((n_y, 7, SPAN), f32)],
        axis=1,
    )
    small = jnp.concatenate(two_parts(small), axis=2)
    grads = jnp.einsum("tr,tc->rc", tokens, d_pre, preferred_element_type=f32)
    piece = model // (n_y * n_z)
    grads = grads.astype(bf16).reshape(n_z, n_y, piece, 2 * owned)
    grads = grads.transpose(1, 0, 2, 3).reshape(n_y, n_z * piece, 2 * owned)
    arrived = exchange(jnp.concatenate([grads, small], axis=1), "y").astype(f32)
    arrived = jnp.sum(arrived, axis=0)
    grads = arrived[: n_z * piece].astype(bf16).reshape(n_z, piece, 2 * owned)
    small = arrived[n_z * piece :]
    small = small[:, :SPAN] + small[:, SPAN:]
    line_high, line_low = two_parts(small[part : part + 1])
    half = part // 2
    small = jnp.concatenate(
        [
            jnp.concatenate([small[:half], small[half:part]], axis=1).astype(bf16),
            jnp.concatenate([line_high, line_low], axis=1),
            jnp.zeros((3, 2 * SPAN), bf16),
        ]
    )
    small = jnp.broadcast_to(small, (n_z, *small.shape))
    arrived = exchange(jnp.concatenate([grads, small], axis=1), "z").astype(f32)
    arrived = jnp.sum(arrived, axis=0) * loss_scale
    grad_carry = arrived[:piece, :owned]
    grad_gate = arrived[:piece, owned:]
    small = arrived[piece:]
    line = small[half : half + 1]
    small = jnp.concatenate(
        [
            small[:half, :SPAN],
            small[:half, SPAN:],
            line[:, :SPAN] + line[:, SPAN:],
            jnp.zeros((7, SPAN), f32),
        ]
    )
    small = to_all(small, "y")
    lines = small[:, part]
    seen = small[:, :part].reshape(n_y * part, SPAN)
    corner = seen[SEGMENT:]
    corner = jnp.concatenate([corner[:, :SEGMENT], corner[:, SEGMENT:]])
    corner = jnp.concatenate([corner, jnp.zeros_like(corner)], axis=1)
    grad_mix = jnp.concatenate([corner, seen[:SEGMENT]])[None]
    grad_bias = lines[:1]
    grad_gain = lines[1]
    grad_shift = lines[2]

    partial = jnp.einsum("tc,dc->td", d_carry_pre, w_carry, preferred_element_type=f32)
    partial = partial + jnp.einsum("tc,dc->td", d_gate_pre, w_gate, preferred_element_type=f32)
    partial = partial.astype(bf16)
    core = lax.axis_index("c")
    low, high = partial[:, : model // 2], partial[:, model // 2 :]
    mine = jnp.where(core == 0, low, high)
    theirs = lax.ppermute(jnp.where(core == 0, high, low), "c", SWAP)
    pair = (mine.astype(f32) + theirs.astype(f32)).astype(bf16)
    pair = exchange(pair.reshape(n_x, rows // n_x, model // 2), "x")
    final = jnp.sum(pair.astype(f32), axis=0).astype(bf16)
    final = to_all(final, DP).reshape(n_x, 2, rows // n_x, model // 2)
    grad_input = final.transpose(0, 2, 1, 3).reshape(rows, model)
    return grad_input, grad_carry, grad_gate, grad_mix, grad_bias, grad_gain, grad_shift


def solution(mesh):
    finer = Mesh(mesh.devices.reshape(16, 4, 4, 2), ("z", "y", "x", "c"))
    placed = (
        P(SP, None),
        P(None, DP),
        P(None, DP),
        P(DP, None, None),
        P(DP, None),
        P(DP),
        P(DP),
        P(SP, DP),
    )
    return jax.shard_map(
        shards,
        mesh=finer,
        in_specs=placed,
        out_specs=(
            P(SP, None),
            P(SP, DP),
            P(SP, DP),
            P(DP, None, None),
            P(DP, None),
            P(DP),
            P(DP),
        ),
        check_vma=False,
    )
```

time: 156 us -> 127 us (0.81)
  the two profiles are of different devices: /device:TPU:8 before, /device:TPU:64 now
where the time goes in v1:
time: 127 us; the launch traced here: 126 us
  waiting for transfers between devices  63.9 us (50%)
  starting transfers between devices  35.8 us (28%)
  local copies, waits for them, and re-layouts  11.1 us (9%)
  matrix products  8.05 us (6%)
  other arithmetic  6.37 us (5%)
    all_to_all x6, waiting for transfers between devices, exchange(): return lax.all_to_all(tiles, axes, split_axis=0, concat_axis=0, tiled=True)  62 us
    all_to_all x6, starting transfers between devices, exchange(): return lax.all_to_all(tiles, axes, split_axis=0, concat_axis=0, tiled=True)  33.8 us
  transfers between devices with their start and end apart: 7, of which 7 were waited for; matrix products, arithmetic and copies ran while one was open for 6% of the time, Pallas kernels for 0%

profile of v1, /device:TPU:64, one launch (start us, length us, event | category | flops | bytes accessed | tf_op | source)
XLA Modules:
  0.0 126.1 jit_solution(15314397029333106369)
XLA Ops:
  0.7 1.2 copy-done
  1.9 1.9 %fusion.60 = (f32[256]{0:T(256)S(1)}, f32[256,128]{1,0:T(8,128)S(1)}, f32[256,128]{1,0:T(8,128)S(1)}) fusion(bf16[256,128]{1,0:T(8,128)(2,1)} %param.15, bf16[256,2048]{1,0:T(8,128)(2,1)S(1)} %copy-done, bf16[2048,128]{1,0:T(8,128)(2,1)} %param.9), kind=kOutput, calls=%fused_computation.140 | convolution fusion | flops 136478464 | bytes 1901568 | tf_op jit(solution)/shard_map/dot_general | solution.py:58
  3.8 0.5 fusion.24
  4.3 0.8 fusion.61
  5.0 0.3 multiply_reduce_fusion.1
  5.3 0.6 broadcast_in_dim.18
  5.9 4.3 %all-to-all-start = ((f32[8,8,128]{2,1,0:T(8,128)}), f32[8,8,128]{2,1,0:T(8,128)S(1)}, u32[]{:S(2)}, u32[]{:S(2)}) async-start(f32[8,8,128]{2,1,0:T(8,128)} %broadcast_in_dim.18), calls=%async_computation | async-start | bytes 65536 | tf_op jit(solution)/shard_map/all_to_all | solution.py:24
  10.4 0.1 pad.21.clone
  10.5 5.2 %all-to-all-done = f32[8,8,128]{2,1,0:T(8,128)S(1)} async-done(((f32[8,8,128]{2,1,0:T(8,128)}), f32[8,8,128]{2,1,0:T(8,128)S(1)}, u32[]{:S(2)}, u32[]{:S(2)}) %all-to-all-start) | async-done | bytes 32800 | tf_op jit(solution)/shard_map/all_to_all | solution.py:24
  15.8 0.2 fusion.23
  16.0 0.3 convolution_bitcast_fusion
  16.4 0.3 convolution_add_fusion.1
  16.7 0.1 fusion.5
  16.8 1.5 %fusion.69 = f32[256,2048]{1,0:T(8,128)S(1)} fusion(bf16[256,128]{1,0:T(8,128)(2,1)S(1)} %fusion.5, bf16[2048,128]{1,0:T(8,128)(2,1)} %param.9), kind=kOutput, calls=%fused_computation.148 | convolution fusion | flops 134217728 | bytes 2686976 | tf_op jit(solution)/shard_map/tc,dc->td/dot_general | solution.py:162
  18.2 1.4 %fusion.1 = bf16[2048,256]{0,1:T(8,128)(2,1)} fusion(bf16[256,2048]{1,0:T(8,128)(2,1)S(1)} %copy-done, bf16[256,128]{1,0:T(8,128)(2,1)S(1)} %get-tuple-element.24, bf16[256,128]{1,0:T(8,128)(2,1)S(1)} %fusion.5), kind=kOutput, calls=%fused_computation.3 | convolution fusion | flops 269221888 | bytes 2228224 | tf_op jit(solution)/shard_map/tr,tc->rc/dot_general | solution.py:118
  19.7 2.3 %copy.37 = bf16[2048,256]{1,0:T(8,128)(2,1)} copy(bf16[2048,256]{0,1:T(8,128)(2,1)} %fusion.1) | data formatting | bytes 2097152 | tf_op jit(solution)/shard_map/convert_element_type | solution.py:120
  21.9 1.3 %copy.38 = bf16[4,16,32,256]{3,2,1,0:T(8,128)(2,1)S(1)} copy(bf16[4,16,32,256]{3,2,0,1:T(8,128)(2,1)} %bitcast.99) | data formatting | bytes 2097152 | tf_op jit(solution)/shard_map/transpose | solution.py:121
  23.3 0.1 maximum_maximum_fusion.2
  23.4 0.1 reduce-precision_convert_fusion
  23.5 1.1 maximum_maximum_fusion
  24.6 4.5 %all-to-all-start.3 = ((bf16[4,544,256]{2,1,0:T(8,128)(2,1)}), bf16[4,544,256]{2,1,0:T(8,128)(2,1)}, u32[]{:S(2)}, u32[]{:S(2)}) async-start(bf16[4,544,256]{2,1,0:T(8,128)(2,1)} %maximum_maximum_fusion), calls=%async_computation.3 | async-start | bytes 2228224 | tf_op jit(solution)/shard_map/all_to_all | solution.py:24
  29.1 1.5 %fusion = bf16[256,2048]{1,0:T(8,128)(2,1)S(1)} fusion(f32[256,2048]{1,0:T(8,128)S(1)} %fusion.69, bf16[256,128]{1,0:T(8,128)(2,1)S(1)} %get-tuple-element.24, bf16[2048,128]{1,0:T(8,128)(2,1)} %param.10), kind=kOutput, calls=%fused_computation.1 | convolution fusion | flops 135266304 | bytes 3735552 | tf_op jit(solution)/shard_map/tc,dc->td/dot_general | solution.py:163
  30.7 1.9 %collective-permute-start = (bf16[256,1024]{1,0:T(8,128)(2,1)S(1)}, bf16[256,1024]{1,0:T(8,128)(2,1)S(1)}, u32[]{:S(2)}, u32[]{:S(2)}) collective-permute-start(bf16[256,1024]{1,0:T(8,128)(2,1)S(1)} %broadcast_select_fusion), channel_id=1, source_target_pairs={{0,1},{1,0},{2,3},{3,2},{4,5},{5,4},{6,7},{7,6},{8,9},{9,8},{10,11... | collective-permute-start | bytes 1572872 | tf_op jit(solution)/shard_map/ppermute | solution.py:168
  32.6 1.9 %collective-permute-done = bf16[256,1024]{1,0:T(8,128)(2,1)S(1)} collective-permute-done((bf16[256,1024]{1,0:T(8,128)(2,1)S(1)}, bf16[256,1024]{1,0:T(8,128)(2,1)S(1)}, u32[]{:S(2)}, u32[]{:S(2)}) %collective-permute-start) | collective-permute-done | bytes 524320 | tf_op jit(solution)/shard_map/ppermute | solution.py:168
  34.5 1.1 add_convert_fusion
  35.5 9.5 %all-to-all-done.3 = bf16[4,544,256]{2,1,0:T(8,128)(2,1)} async-done(((bf16[4,544,256]{2,1,0:T(8,128)(2,1)}), bf16[4,544,256]{2,1,0:T(8,128)(2,1)}, u32[]{:S(2)}, u32[]{:S(2)}) %all-to-all-start.3) | async-done | bytes 1114144 | tf_op jit(solution)/shard_map/all_to_all | solution.py:24
  45.0 3.5 %all-to-all-start.1 = ((bf16[4,64,1024]{2,1,0:T(8,128)(2,1)}), bf16[4,64,1024]{2,1,0:T(8,128)(2,1)S(1)}, u32[]{:S(2)}, u32[]{:S(2)}) async-start(bf16[4,64,1024]{2,1,0:T(8,128)(2,1)} %bitcast.16), calls=%async_computation.1 | async-start | bytes 1048576 | tf_op jit(solution)/shard_map/all_to_all | solution.py:24
  48.5 0.1 pad.15.clone
  48.6 1.5 %convert_reduce_fusion = f32[544,256]{1,0:T(8,128)S(1)} fusion(bf16[4,544,256]{2,1,0:T(8,128)(2,1)} %all-to-all-done.3), kind=kLoop, calls=%fused_computation.4 | loop fusion | flops 974848 | bytes 1671168 | tf_op jit(solution)/shard_map/reduce_sum | solution.py:123
  50.0 7.0 %all-to-all-done.1 = bf16[4,64,1024]{2,1,0:T(8,128)(2,1)S(1)} async-done(((bf16[4,64,1024]{2,1,0:T(8,128)(2,1)}), bf16[4,64,1024]{2,1,0:T(8,128)(2,1)S(1)}, u32[]{:S(2)}, u32[]{:S(2)}) %all-to-all-start.1) | async-done | bytes 524320 | tf_op jit(solution)/shard_map/all_to_all | solution.py:24
  57.0 0.1 reduce_sum.164
  57.1 1.1 broadcast_in_dim.19
  58.2 3.6 %all-to-all-start.2 = ((bf16[8,64,1024]{2,1,0:T(8,128)(2,1)}), bf16[8,64,1024]{2,1,0:T(8,128)(2,1)S(1)}, u32[]{:S(2)}, u32[]{:S(2)}) async-start(bf16[8,64,1024]{2,1,0:T(8,128)(2,1)} %broadcast_in_dim.19), calls=%async_computation.2 | async-start | bytes 2097152 | tf_op jit(solution)/shard_map/all_to_all | solution.py:24
  61.8 0.1 maximum_maximum_fusion.4
  61.9 0.8 pad_maximum_fusion
  62.7 15.0 %all-to-all-done.2 = bf16[8,64,1024]{2,1,0:T(8,128)(2,1)S(1)} async-done(((bf16[8,64,1024]{2,1,0:T(8,128)(2,1)}), bf16[8,64,1024]{2,1,0:T(8,128)(2,1)S(1)}, u32[]{:S(2)}, u32[]{:S(2)}) %all-to-all-start.2) | async-done | bytes 1048608 | tf_op jit(solution)/shard_map/all_to_all | solution.py:24
  77.6 14.8 %all-to-all-start.4 = ((bf16[16,48,256]{2,1,0:T(8,128)(2,1)}), bf16[16,48,256]{2,1,0:T(8,128)(2,1)S(1)}, u32[]{:S(2)}, u32[]{:S(2)}) async-start(bf16[16,48,256]{2,1,0:T(8,128)(2,1)} %pad_maximum_fusion), calls=%async_computation.4 | async-start | bytes 786432 | tf_op jit(solution)/shard_map/all_to_all | solution.py:24
  92.4 1.1 copy.36
  93.5 1.2 copy.47
  94.7 20.4 %all-to-all-done.4 = bf16[16,48,256]{2,1,0:T(8,128)(2,1)S(1)} async-done(((bf16[16,48,256]{2,1,0:T(8,128)(2,1)}), bf16[16,48,256]{2,1,0:T(8,128)(2,1)S(1)}, u32[]{:S(2)}, u32[]{:S(2)}) %all-to-all-start.4) | async-done | bytes 393248 | tf_op jit(solution)/shard_map/all_to_all | solution.py:24
  115.2 0.1 maximum_maximum_fusion.3
  115.3 0.6 broadcast_in_dim.49
  115.9 3.3 %all-to-all-start.5 = ((f32[4,32,128]{2,1,0:T(8,128)}), f32[4,32,128]{2,1,0:T(8,128)S(1)}, u32[]{:S(2)}, u32[]{:S(2)}) async-start(f32[4,32,128]{2,1,0:T(8,128)} %broadcast_in_dim.49), calls=%async_computation.5 | async-start | bytes 131072 | tf_op jit(solution)/shard_map/all_to_all | solution.py:24
  119.2 0.6 fusion.66
  119.8 5.0 %all-to-all-done.5 = f32[4,32,128]{2,1,0:T(8,128)S(1)} async-done(((f32[4,32,128]{2,1,0:T(8,128)}), f32[4,32,128]{2,1,0:T(8,128)S(1)}, u32[]{:S(2)}, u32[]{:S(2)}) %all-to-all-start.5) | async-done | bytes 65568 | tf_op jit(solution)/shard_map/all_to_all | solution.py:24
  124.8 0.1 fusion.64
  124.9 0.6 maximum_bitcast_fusion
  125.6 0.5 slice_bitcast_fusion
  (47 shorter events, 0.6 us)
Async XLA Ops:
  0.6 1.2 copy-start
  1.9 1.9 %copy-start.3 = (bf16[1,128,128]{2,1,0:T(8,128)(2,1)S(1)}, bf16[1,128,128]{2,1,0:T(8,128)(2,1)}, u32[]{:S(2)}) copy-start(bf16[1,128,128]{2,1,0:T(8,128)(2,1)} %param.11) | copy-start | bytes 98308
  1.9 1.9 %copy-start.5 = (f32[128]{0:T(128)S(1)}, f32[128]{0:T(128)}, u32[]{:S(2)}) copy-start(f32[128]{0:T(128)} %param.13) | copy-start | bytes 1540
  1.9 2.4 %copy-start.1 = (bf16[2048,128]{1,0:T(8,128)(2,1)S(1)}, bf16[2048,128]{1,0:T(8,128)(2,1)}, u32[]{:S(2)}) copy-start(bf16[2048,128]{1,0:T(8,128)(2,1)} %param.10) | copy-start | bytes 1572868
  4.2 11.6 %copy-start.7 = (f32[128]{0:T(128)S(1)}, f32[128]{0:T(128)}, u32[]{:S(2)}) copy-start(f32[128]{0:T(128)} %param.14) | copy-start | bytes 1540
  4.3 12.1 %copy-start.6 = (f32[1,128]{1,0:T(1,128)S(1)}, f32[1,128]{1,0:T(1,128)}, u32[]{:S(2)}) copy-start(f32[1,128]{1,0:T(1,128)} %param.12) | copy-start | bytes 1540
  5.0 11.6 %copy-start.4 = (bf16[256,128]{1,0:T(8,128)(2,1)S(1)}, bf16[256,128]{1,0:T(8,128)(2,1)}, u32[]{:S(2)}) copy-start(bf16[256,128]{1,0:T(8,128)(2,1)} %param.15) | copy-start | bytes 196612
  5.9 9.7 %all-to-all-start = ((f32[8,8,128]{2,1,0:T(8,128)}), f32[8,8,128]{2,1,0:T(8,128)S(1)}, u32[]{:S(2)}, u32[]{:S(2)}) async-start(f32[8,8,128]{2,1,0:T(8,128)} %broadcast_in_dim.18), calls=%async_computation | async-start | bytes 65536 | tf_op jit(solution)/shard_map/all_to_all | solution.py:24
  16.3 3.4 %copy-start.2 = (f32[128,128]{1,0:T(8,128)}, f32[128,128]{1,0:T(8,128)S(1)}, u32[]{:S(2)}) copy-start(f32[128,128]{1,0:T(8,128)S(1)} %convolution_bitcast_fusion) | copy-start | bytes 196612
  21.9 1.3 %slice-start = ((f32[128,128]{1,0:T(8,128)}), f32[64,128]{1,0:T(8,128)S(1)}, s32[]{:S(2)}) async-start(f32[128,128]{1,0:T(8,128)} %copy-done.2), calls=%async_computation.6 | async-start | bytes 65536 | tf_op jit(solution)/shard_map/slice | solution.py:107
  24.6 20.3 %all-to-all-start.3 = ((bf16[4,544,256]{2,1,0:T(8,128)(2,1)}), bf16[4,544,256]{2,1,0:T(8,128)(2,1)}, u32[]{:S(2)}, u32[]{:S(2)}) async-start(bf16[4,544,256]{2,1,0:T(8,128)(2,1)} %maximum_maximum_fusion), calls=%async_computation.3 | async-start | bytes 2228224 | tf_op jit(solution)/shard_map/all_to_all | solution.py:24
  30.7 3.8 %collective-permute-start = (bf16[256,1024]{1,0:T(8,128)(2,1)S(1)}, bf16[256,1024]{1,0:T(8,128)(2,1)S(1)}, u32[]{:S(2)}, u32[]{:S(2)}) collective-permute-start(bf16[256,1024]{1,0:T(8,128)(2,1)S(1)} %broadcast_select_fusion), channel_id=1, source_target_pairs={{0,1},{1,0},{2,3},{3,2},{4,5},{5,4},{6,7},{7,6},{8,9},{9,8},{10,11... | collective-permute-start | bytes 1572872 | tf_op jit(solution)/shard_map/ppermute | solution.py:168
  45.0 12.0 %all-to-all-start.1 = ((bf16[4,64,1024]{2,1,0:T(8,128)(2,1)}), bf16[4,64,1024]{2,1,0:T(8,128)(2,1)S(1)}, u32[]{:S(2)}, u32[]{:S(2)}) async-start(bf16[4,64,1024]{2,1,0:T(8,128)(2,1)} %bitcast.16), calls=%async_computation.1 | async-start | bytes 1048576 | tf_op jit(solution)/shard_map/all_to_all | solution.py:24
  58.2 19.4 %all-to-all-start.2 = ((bf16[8,64,1024]{2,1,0:T(8,128)(2,1)}), bf16[8,64,1024]{2,1,0:T(8,128)(2,1)S(1)}, u32[]{:S(2)}, u32[]{:S(2)}) async-start(bf16[8,64,1024]{2,1,0:T(8,128)(2,1)} %broadcast_in_dim.19), calls=%async_computation.2 | async-start | bytes 2097152 | tf_op jit(solution)/shard_map/all_to_all | solution.py:24
  77.6 37.5 %all-to-all-start.4 = ((bf16[16,48,256]{2,1,0:T(8,128)(2,1)}), bf16[16,48,256]{2,1,0:T(8,128)(2,1)S(1)}, u32[]{:S(2)}, u32[]{:S(2)}) async-start(bf16[16,48,256]{2,1,0:T(8,128)(2,1)} %pad_maximum_fusion), calls=%async_computation.4 | async-start | bytes 786432 | tf_op jit(solution)/shard_map/all_to_all | solution.py:24
  115.9 8.9 %all-to-all-start.5 = ((f32[4,32,128]{2,1,0:T(8,128)}), f32[4,32,128]{2,1,0:T(8,128)S(1)}, u32[]{:S(2)}, u32[]{:S(2)}) async-start(f32[4,32,128]{2,1,0:T(8,128)} %broadcast_in_dim.49), calls=%async_computation.5 | async-start | bytes 131072 | tf_op jit(solution)/shard_map/all_to_all | solution.py:24

commit v2 on v1

v2 whole, which is shorter than its diff:
```python
import math

import jax
import jax.numpy as jnp
from jax import lax
from jax.experimental import pallas as pl
from jax.experimental.pallas import tpu as pltpu
from jax.sharding import Mesh
from jax.sharding import PartitionSpec as P

SPAN = 128
SEGMENT = 64
SP = ("z", "y")
DP = ("x", "c")
SWAP = ((0, 1), (1, 0))

sqrt_half = 0.7071067811865476
density = 0.3989422804014327
epsilon = 1e-06
bf16 = jnp.bfloat16
f32 = jnp.float32
highest = lax.Precision.HIGHEST


def exchange(tiles, axes):
    return lax.all_to_all(tiles, axes, split_axis=0, concat_axis=0, tiled=True)


def ahead(value, axis, k):
    n = lax.axis_size(axis)
    return lax.ppermute(value, axis, [(i, (i + k) % n) for i in range(n)])


def call(body, outs, *args, flops=1, scalars=0, scratch=(), moved=1):
    smem = pl.BlockSpec(memory_space=pltpu.SMEM)
    vmem = pl.BlockSpec(memory_space=pltpu.VMEM)
    return pl.pallas_call(
        body,
        out_shape=[jax.ShapeDtypeStruct(s, d) for s, d in outs],
        in_specs=[smem] * scalars + [vmem] * (len(args) - scalars),
        out_specs=[vmem] * len(outs),
        scratch_shapes=list(scratch),
        cost_estimate=pl.CostEstimate(flops=flops, bytes_accessed=moved, transcendentals=0),
    )(*args)


def dot(a, b, precision=None):
    return lax.dot_general(
        a, b, (((1,), (0,)), ((), ())), precision=precision, preferred_element_type=f32
    )


def dot_t(a, b, precision=None):
    return lax.dot_general(
        a, b, (((1,), (1,)), ((), ())), precision=precision, preferred_element_type=f32
    )


def visible(weights):
    t = lax.broadcasted_iota(jnp.int32, (SPAN, SPAN), 0)
    s = lax.broadcasted_iota(jnp.int32, (SPAN, SPAN), 1)
    return jnp.where(t // SEGMENT >= s // SEGMENT, weights.astype(f32), 0.0)


def gelu(v):
    return 0.5 * v * (1.0 + lax.erf(v * sqrt_half))


def gelu_slope(v):
    return 0.5 * (1.0 + lax.erf(v * sqrt_half)) + v * jnp.exp(-0.5 * v * v) * density


def local_part(tok, wc, wg, mix, gain, cot, carry, gate, act, ds, dg, stats, acc_c, acc_g):
    step = pl.program_id(0)

    @pl.when(step == 0)
    def _():
        acc_c[...] = jnp.zeros_like(acc_c)
        acc_g[...] = jnp.zeros_like(acc_g)

    acc_c[...] += dot(tok[...], wc[...])
    acc_g[...] += dot(tok[...], wg[...])

    @pl.when(step == pl.num_programs(0) - 1)
    def _():
        carry[...] = acc_c[...].astype(bf16)
        gate[...] = acc_g[...].astype(bf16)
        owned = wc.shape[1]
        weights = visible(mix[0])
        ones = jnp.ones((8, owned), f32)
        rows = []
        for b in range(tok.shape[0] // SPAN):
            here = pl.ds(b * SPAN, SPAN)
            a = gelu(gate[here, :].astype(f32))
            act[here, :] = a
            d = cot[here, :].astype(f32) * gelu(carry[here, :].astype(f32))
            ds[here, :] = d
            back = lax.dot_general(
                weights, d, (((0,), (0,)), ((), ())), precision=highest, preferred_element_type=f32
            )
            dg[here, :] = back
            n = back * gain[...]
            off_a = a - jnp.mean(a, axis=1, keepdims=True)
            off_n = n - jnp.mean(n, axis=1, keepdims=True)
            rows.append(
                (
                    dot_t(ones, a, highest)[:1] / owned,
                    dot_t(ones, n, highest)[:1] / owned,
                    dot_t(ones, off_a * off_a, highest)[:1],
                    dot_t(ones, off_a * off_n, highest)[:1],
                )
            )
        table = jnp.concatenate([r[k] for k in range(4) for r in rows], axis=0)
        for j in range(stats.shape[0]):
            stats[j] = table


def turned(tok, carry, gate, cot, turned_tok, slope_c, slope_g):
    n_y = turned_tok.shape[0]
    piece = 32
    wide = 8 * piece * n_y // 2
    for at in range(0, tok.shape[1], wide):
        block = jnp.transpose(tok[:, at : at + wide])
        for q in range(wide // piece):
            k = at // piece + q
            turned_tok[k % n_y, pl.ds(k // n_y * piece, piece), :] = block[q * piece : q * piece + piece]
    slope_c[...] = cot[...].astype(f32) * gelu_slope(carry[...].astype(f32))
    slope_g[...] = gelu_slope(gate[...].astype(f32))


def normal_part(
    stats, act, ds, dg, slope_c, slope_g, mix, bias, gain, shift, tok_t, sent, d_pre
):
    n, owned = stats.shape[0], act.shape[1]
    st = stats[...]
    mean = jnp.sum(st, axis=0) / n
    dev = st[:, 0:4] - mean[None, 0:4]
    dev_a, dev_d = dev[:, 0:2], dev[:, 2:4]
    square = n * mean[4:6] + owned * jnp.sum(dev_a * dev_a, axis=0)
    cross = n * mean[6:8] + owned * jnp.sum(dev_a * dev_d, axis=0)
    rstd = lax.rsqrt(square / (n * owned) + epsilon)
    table = jnp.concatenate([mean[0:4], rstd, rstd * cross / (n * owned)], axis=0)
    table = jnp.transpose(table)
    weights = visible(mix[0])
    bias_col = jnp.transpose(jnp.broadcast_to(bias[...], (8, SPAN)))[:, 0:1]
    mix_sum = jnp.zeros((SPAN, SPAN), f32)
    gain_sum = jnp.zeros((1, owned), f32)
    shift_sum = jnp.zeros((1, owned), f32)
    ds_sum = jnp.zeros((SPAN, owned), f32)
    for b in range(2):
        here = pl.ds(b * SPAN, SPAN)
        inv = table[:, 4 + b : 5 + b]
        normed = (act[here, :] - table[:, b : b + 1]) * inv
        gated = normed * gain[...] + shift[...]
        spatial = dot(weights, gated, highest) + bias_col
        d_pre[here, 0:owned] = (slope_c[here, :] * spatial).astype(bf16)
        back = dg[here, :]
        d_act = inv * (
            back * gain[...] - table[:, 2 + b : 3 + b] - normed * table[:, 6 + b : 7 + b]
        )
        d_pre[here, owned:] = (d_act * slope_g[here, :]).astype(bf16)
        d = ds[here, :]
        mix_sum += dot_t(d, gated, highest)
        ds_sum += d
        gain_sum += jnp.sum(back * normed, axis=0, keepdims=True)
        shift_sum += jnp.sum(back, axis=0, keepdims=True)
    bias_sum = dot_t(jnp.ones((8, owned), f32), ds_sum, highest)[:1]
    lane = lax.broadcasted_iota(jnp.int32, (SEGMENT // 2, SPAN), 1)
    corner = jnp.where(
        lane < SEGMENT,
        mix_sum[: SEGMENT // 2],
        pltpu.roll(mix_sum[SEGMENT // 2 : SEGMENT], SEGMENT, 1),
    )
    seen = jnp.concatenate([mix_sum[SEGMENT:], corner], axis=0)
    row = lax.broadcasted_iota(jnp.int32, (8, SPAN), 0)
    lines = (bias_sum, gain_sum, shift_sum, jnp.zeros_like(bias_sum))
    grads_at = tok_t.shape[1]
    part = seen.shape[0] // sent.shape[0]
    for j in range(sent.shape[0]):
        line = jnp.where(row == 0, jnp.broadcast_to(lines[j], (8, SPAN)), 0.0)
        small = jnp.concatenate([seen[j * part : j * part + part], line], axis=0)
        high = small.astype(bf16)
        sent[j, grads_at:, 0:SPAN] = high
        sent[j, grads_at:, SPAN:] = (small - high.astype(f32)).astype(bf16)
    for j in range(sent.shape[0]):
        sent[j, 0:grads_at, :] = dot(tok_t[j], d_pre[...]).astype(bf16)


def summed_y(came, sent):
    n_z = sent.shape[0]
    piece = 32
    grads_at = n_z * piece
    total = came[0].astype(f32)
    for j in range(1, came.shape[0]):
        total = total + came[j].astype(f32)
    small = total[grads_at:, 0:SPAN] + total[grads_at:, SPAN:]
    row = lax.broadcasted_iota(jnp.int32, (8, SPAN), 0)
    line = jnp.broadcast_to(small[24:25], (8, SPAN))
    high = line.astype(bf16).astype(f32)
    line = jnp.where(row == 0, high, jnp.where(row == 1, line - high, 0.0))
    right = jnp.concatenate([small[16:24], line], axis=0)
    small = jnp.concatenate([small[0:16], right], axis=1).astype(bf16)
    for k in range(n_z):
        sent[k, 0:piece, :] = total[k * piece : k * piece + piece].astype(bf16)
        sent[k, piece:, :] = small


def summed_z(came, carry, gate, small, *, scale):
    total = came[0].astype(f32)
    for k in range(1, came.shape[0]):
        total = total + came[k].astype(f32)
    total = total * scale
    owned = carry.shape[1]
    carry[...] = total[0:32, 0:owned]
    gate[...] = total[0:32, owned:]
    row = lax.broadcasted_iota(jnp.int32, (8, SPAN), 0)
    line = jnp.broadcast_to(total[40:41, SPAN:] + total[41:42, SPAN:], (8, SPAN))
    line = jnp.where(row == 0, line, 0.0)
    part = jnp.concatenate([total[32:48, 0:SPAN], total[32:40, SPAN:], line], axis=0)
    for j in range(small.shape[0]):
        small[j] = part


def unpacked(small, mix, bias, gain, shift):
    lane = lax.broadcasted_iota(jnp.int32, (SEGMENT // 2, SPAN), 1)
    corner = jnp.concatenate([small[2, 16:24], small[3, 0:24]], axis=0)
    mix[0, 0 : SEGMENT // 2, :] = jnp.where(lane < SEGMENT, corner, 0.0)
    mix[0, SEGMENT // 2 : SEGMENT, :] = jnp.where(
        lane < SEGMENT, pltpu.roll(corner, SEGMENT, 1), 0.0
    )
    mix[0, 64:88, :] = small[0, 0:24]
    mix[0, 88:112, :] = small[1, 0:24]
    mix[0, 112:128, :] = small[2, 0:16]
    bias[...] = small[0, 24:25]
    gain[...] = small[1, 24:25]
    shift[...] = small[2, 24:25]


def theirs_part(at, d_pre, wc, wg, out):
    owned = wc.shape[1]
    half = out.shape[0]
    rows = d_pre[pl.ds(pl.multiple_of((1 - at[0]) * half, half), half), :]
    for n in range(0, out.shape[1], 512):
        here = pl.ds(n, 512)
        v = dot_t(rows[:, :owned], wc[here, :]) + dot_t(rows[:, owned:], wg[here, :])
        out[:, n : n + 512] = v.astype(bf16)


def pair_part(at, d_pre, wc, wg, came, own, one, two, three, held):
    owned = wc.shape[1]
    half, piece = held.shape[0], own.shape[0]
    rows = d_pre[pl.ds(pl.multiple_of(at[0] * half, half), half), :]
    for n in range(0, own.shape[1], 512):
        here = pl.ds(n, 512)
        v = dot_t(rows[:, :owned], wc[here, :]) + dot_t(rows[:, owned:], wg[here, :])
        held[:, n : n + 512] = v + came[:, n : n + 512].astype(f32)
    for k, out in enumerate((own, one, two, three)):
        first = pl.multiple_of(((at[1] + k) & 3) * piece, piece)
        out[...] = held[pl.ds(first, piece), :].astype(out.dtype)


def summed_x(own, one, two, three, out):
    total = own[...] + one[...].astype(f32) + two[...].astype(f32) + three[...].astype(f32)
    out[...] = total.astype(bf16)


def joined_x(at, own, one, two, three, out):
    piece = own.shape[0]
    for k, part in enumerate((own, one, two, three)):
        first = pl.multiple_of(((at[1] + 4 - k) & 3) * piece, piece)
        out[pl.ds(first, piece), :] = part[...]


def joined_pair(at, own, other, out):
    half = own.shape[0]
    out[pl.ds(pl.multiple_of(at[0] * half, half), half), :] = own[...]
    out[pl.ds(pl.multiple_of((1 - at[0]) * half, half), half), :] = other[...]


def shards(tokens, w_carry, w_gate, mix_weight, mix_bias, ln_gain, ln_shift, cotangent):
    rows, model = tokens.shape
    owned = w_carry.shape[1]
    n_dp = lax.axis_size(DP)
    n_x, n_y, n_z = lax.axis_size("x"), lax.axis_size("y"), lax.axis_size("z")
    loss_scale = 1.0 / math.sqrt(rows * n_y * n_z)
    gain, shift = ln_gain.reshape(1, owned), ln_shift.reshape(1, owned)
    at = jnp.stack([lax.axis_index("c"), lax.axis_index("x")]).astype(jnp.int32)

    steps = 4
    deep = model // steps
    whole = lambda shape: pl.BlockSpec(shape, lambda k: (0,) * len(shape))
    act_shape = jax.ShapeDtypeStruct((rows, owned), f32)
    carry, gate, act, ds, dg, stats = pl.pallas_call(
        local_part,
        grid=(steps,),
        in_specs=[
            pl.BlockSpec((rows, deep), lambda k: (0, k)),
            pl.BlockSpec((deep, owned), lambda k: (k, 0)),
            pl.BlockSpec((deep, owned), lambda k: (k, 0)),
            whole((1, SPAN, SPAN)),
            whole((1, owned)),
            whole((rows, owned)),
        ],
        out_specs=[whole((rows, owned))] * 5 + [whole((n_dp, 8, SPAN))],
        out_shape=[
            jax.ShapeDtypeStruct((rows, owned), bf16),
            jax.ShapeDtypeStruct((rows, owned), bf16),
            act_shape,
            act_shape,
            act_shape,
            jax.ShapeDtypeStruct((n_dp, 8, SPAN), f32),
        ],
        scratch_shapes=[pltpu.VMEM((rows, owned), f32)] * 2,
    )(tokens, w_carry, w_gate, mix_weight, gain, cotangent)

    stats = exchange(stats, DP)
    tok_t, slope_c, slope_g = call(
        turned,
        [((n_y, model // n_y, rows), bf16), ((rows, owned), f32), ((rows, owned), f32)],
        tokens, carry, gate, cotangent,
        flops=2 * 10**9, moved=2 * rows * model * 2,
    )
    sent, d_pre = call(
        normal_part,
        [((n_y, model // n_y + 32, 2 * owned), bf16), ((rows, 2 * owned), bf16)],
        stats, act, ds, dg, slope_c, slope_g, mix_weight, mix_bias, gain, shift, tok_t,
        flops=10**9, moved=2 * rows * model * 2,
    )

    with jax.named_scope("sum_y"):
        came = exchange(sent, "y")
    (sent,) = call(summed_y, [((n_z, 48, 2 * owned), bf16)], came, flops=10**9, moved=2 * came.size)
    with jax.named_scope("sum_z"):
        came = exchange(sent, "z")
    scaled = lambda *refs: summed_z(*refs, scale=loss_scale)
    piece = model // (n_y * n_z)
    grad_carry, grad_gate, small = call(
        scaled,
        [((piece, owned), f32), ((piece, owned), f32), ((n_y, 32, SPAN), f32)],
        came, flops=10**9, moved=2 * came.size,
    )
    with jax.named_scope("share_y"):
        small = exchange(small, "y")
    grad_mix, grad_bias, grad_gain, grad_shift = call(
        unpacked,
        [((1, SPAN, SPAN), f32), ((1, SPAN), f32), ((1, owned), f32), ((1, owned), f32)],
        small, flops=10**8, moved=4 * small.size,
    )

    half = rows // 2
    part = half // n_x
    (theirs,) = call(
        theirs_part, [((half, model), bf16)], at, d_pre, w_carry, w_gate,
        scalars=1, flops=10**9, moved=4 * half * model,
    )
    with jax.named_scope("pair_sum"):
        theirs = lax.ppermute(theirs, "c", SWAP)
    own, one, two, three = call(
        pair_part,
        [((part, model), f32)] + [((part, model), bf16)] * 3,
        at, d_pre, w_carry, w_gate, theirs,
        scalars=1, flops=10**9, moved=8 * half * model,
        scratch=[pltpu.VMEM((half, model), f32)],
    )
    with jax.named_scope("sum_x"):
        came = [ahead(v, "x", k) for k, v in ((1, one), (2, two), (3, three))]
    (final,) = call(summed_x, [((part, model), bf16)], own, *came, flops=10**8, moved=4 * own.size)
    with jax.named_scope("share_x"):
        came = [ahead(final, "x", k) for k in (1, 2, 3)]
    (joined,) = call(
        joined_x, [((half, model), bf16)], at, final, *came,
        scalars=1, flops=10**8, moved=4 * half * model,
    )
    with jax.named_scope("share_pair"):
        other = lax.ppermute(joined, "c", SWAP)
    (grad_input,) = call(
        joined_pair, [((rows, model), bf16)], at, joined, other,
        scalars=1, flops=10**8, moved=4 * rows * model,
    )
    return (
        grad_input,
        grad_carry,
        grad_gate,
        grad_mix,
        grad_bias,
        grad_gain.reshape(owned),
        grad_shift.reshape(owned),
    )


def solution(mesh):
    finer = Mesh(mesh.devices.reshape(16, 4, 4, 2), ("z", "y", "x", "c"))
    placed = (
        P(SP, None),
        P(None, DP),
        P(None, DP),
        P(DP, None, None),
        P(DP, None),
        P(DP),
        P(DP),
        P(SP, DP),
    )
    return jax.shard_map(
        shards,
        mesh=finer,
        in_specs=placed,
        out_specs=(
            P(SP, None),
            P(SP, DP),
            P(SP, DP),
            P(DP, None, None),
            P(DP, None),
            P(DP),
            P(DP),
        ),
        check_vma=False,
    )
```

time: 127 us -> 121 us (0.953)
  the two profiles are of different devices: /device:TPU:64 before, /device:TPU:1 now
where the time goes in v2:
time: 121 us; the launch traced here: 120 us
  starting transfers between devices  52.6 us (43%)
  waiting for transfers between devices  32 us (26%)
  Pallas kernels  28.2 us (23%)
  local copies, waits for them, and re-layouts  5.88 us (5%)
    all_to_all x4, starting transfers between devices, exchange(): return lax.all_to_all(tiles, axes, split_axis=0, concat_axis=0, tiled=True)  27.9 us
    pallas_call x10, Pallas kernels, call(): pl.pallas_call(body, out_shape=[jax.ShapeDtypeStruct(s, d) for s, d in ou...  23 us
    all_to_all x4, waiting for transfers between devices, exchange(): return lax.all_to_all(tiles, axes, split_axis=0, concat_axis=0, tiled=True)  18.6 us
    ppermute x6, starting transfers between devices, ahead(): return lax.ppermute(value, axis, [(i, (i + k) % n) for i in range(n)])  17.6 us
    ppermute x6, waiting for transfers between devices, ahead(): return lax.ppermute(value, axis, [(i, (i + k) % n) for i in range(n)])  11.6 us
    unnamed x24, local copies, waits for them, and re-layouts  5.88 us
    pallas_call x1, Pallas kernels, shards(): pl.pallas_call(local_part, grid=(steps,), in_specs=[pl.BlockSpec((rows, d...  5.18 us
    ppermute x1, starting transfers between devices, shards(): theirs = lax.ppermute(theirs, 'c', SWAP)  4.05 us
  transfers between devices with their start and end apart: 12, of which 8 were waited for; matrix products, arithmetic and copies ran while one was open for 0% of the time, Pallas kernels for 13%

profile of v2, /device:TPU:1, one launch (start us, length us, event | category | flops | bytes accessed | tf_op | source)
XLA Modules:
  0.0 120.1 jit_solution(12713527591355125086)
XLA Ops:
  0.6 5.2 %shard_map.135 = (bf16[256,128]{1,0:T(8,128)(2,1)}, bf16[256,128]{1,0:T(8,128)(2,1)}, f32[256,128]{1,0:T(8,128)}, f32[256,128]{1,0:T(8,128)}, f32[256,128]{1,0:T(8,128)}, /*index=5*/f32[8,8,128]{2,1,0:T(8,128)}) custom-call(bf16[256,2048]{1,0:T(8,128)(2,1)} %tok.3, bf16[2048,128]{1,0:T(8,128)(2,1)} %wc.5, bf16[2048,128]{1,0:T(8,128)(2,1)} %wg.5, ...), custom_call_target="tpu_custom_call" | custom-call | tf_op jit(solution)/shard_map/pallas_call | solution.py:293
  5.8 10.1 %all-to-all-start = ((f32[8,8,128]{2,1,0:T(8,128)}), f32[8,8,128]{2,1,0:T(8,128)S(1)}, u32[]{:S(2)}, u32[]{:S(2)}) async-start(f32[8,8,128]{2,1,0:T(8,128)} %get-tuple-element.29), calls=%async_computation | async-start | bytes 65536 | tf_op jit(solution)/shard_map/all_to_all | solution.py:26
  15.9 2.6 %shard_map.136 = (bf16[4,512,256]{2,1,0:T(8,128)(2,1)}, f32[256,128]{1,0:T(8,128)}, f32[256,128]{1,0:T(8,128)}) custom-call(bf16[256,2048]{1,0:T(8,128)(2,1)} %tok.3, bf16[256,128]{1,0:T(8,128)(2,1)} %get-tuple-element.33.carry, bf16[256,128]{1,0:T(8,128)(2,1)} %get-tuple-element.34.gate, bf16[256,128]{1,0:T(8,128)(2,1)} %cot.3), custom_call_target="tpu_custom_call" | custom-call | flops 2000000000 | bytes 2097152 | tf_op jit(solution)/shard_map/pallas_call | solution.py:37
  18.5 2.1 %all-to-all-done.stats = f32[8,8,128]{2,1,0:T(8,128)S(1)} async-done(((f32[8,8,128]{2,1,0:T(8,128)}), f32[8,8,128]{2,1,0:T(8,128)S(1)}, u32[]{:S(2)}, u32[]{:S(2)}) %all-to-all-start) | async-done | bytes 32800 | tf_op jit(solution)/shard_map/all_to_all | solution.py:26
  20.6 0.6 copy-done.10
  21.2 3.8 %shard_map.137 = (bf16[4,544,256]{2,1,0:T(8,128)(2,1)}, bf16[256,256]{1,0:T(8,128)(2,1)}) custom-call(f32[8,8,128]{2,1,0:T(8,128)} %copy-done.10, f32[256,128]{1,0:T(8,128)} %get-tuple-element.30.act, f32[256,128]{1,0:T(8,128)} %get-tuple-element.31.ds, f32[256,128]{1,0:T(8,128)} %get-tuple-element.32.dg, f32[256,128]{1,0:T(8,128)} %get-tuple-element.35.slope_c, ...), custom_call_target="tpu_custom_call" | custom-call | flops 1000000000 | bytes 2097152 | tf_op jit(solution)/shard_map/pallas_call | solution.py:37
  25.1 3.5 %all-to-all-start.1 = ((bf16[4,544,256]{2,1,0:T(8,128)(2,1)}), bf16[4,544,256]{2,1,0:T(8,128)(2,1)S(1)}, u32[]{:S(2)}, u32[]{:S(2)}) async-start(bf16[4,544,256]{2,1,0:T(8,128)(2,1)} %get-tuple-element.43), calls=%async_computation.1 | async-start | bytes 2228224 | tf_op jit(solution)/shard_map/sum_y/all_to_all | solution.py:26
  28.6 15.1 %all-to-all-done.1.came = bf16[4,544,256]{2,1,0:T(8,128)(2,1)S(1)} async-done(((bf16[4,544,256]{2,1,0:T(8,128)(2,1)}), bf16[4,544,256]{2,1,0:T(8,128)(2,1)S(1)}, u32[]{:S(2)}, u32[]{:S(2)}) %all-to-all-start.1) | async-done | bytes 1114144 | tf_op jit(solution)/shard_map/sum_y/all_to_all | solution.py:26
  43.7 1.0 copy-done
  44.7 2.1 %shard_map.143 = bf16[16,48,256]{2,1,0:T(8,128)(2,1)} custom-call(bf16[4,544,256]{2,1,0:T(8,128)(2,1)} %copy-done), custom_call_target="tpu_custom_call" | custom-call | flops 1000000000 | bytes 1114112 | tf_op jit(solution)/shard_map/pallas_call | solution.py:37
  46.8 11.0 %all-to-all-start.2 = ((bf16[16,48,256]{2,1,0:T(8,128)(2,1)}), bf16[16,48,256]{2,1,0:T(8,128)(2,1)S(1)}, u32[]{:S(2)}, u32[]{:S(2)}) async-start(bf16[16,48,256]{2,1,0:T(8,128)(2,1)} %shard_map.143), calls=%async_computation.2 | async-start | bytes 786432 | tf_op jit(solution)/shard_map/sum_z/all_to_all | solution.py:26
  57.9 0.6 pad_add_fusion.at
  58.5 2.5 %shard_map.138 = bf16[128,2048]{1,0:T(8,128)(2,1)} custom-call(s32[2]{0:T(128)} %pad_add_fusion.at, bf16[256,256]{1,0:T(8,128)(2,1)} %get-tuple-element.38.d_pre, bf16[2048,128]{1,0:T(8,128)(2,1)} %wc.5, bf16[2048,128]{1,0:T(8,128)(2,1)} %wg.5), custom_call_target="tpu_custom_call" | custom-call | flops 1000000000 | bytes 1048576 | tf_op jit(solution)/shard_map/pallas_call | solution.py:37
  60.9 4.0 %collective-permute-start = (bf16[128,2048]{1,0:T(8,128)(2,1)}, bf16[128,2048]{1,0:T(8,128)(2,1)S(1)}, u32[]{:S(2)}, u32[]{:S(2)}) collective-permute-start(bf16[128,2048]{1,0:T(8,128)(2,1)} %shard_map.138), channel_id=1, source_target_pairs={{0,1},{1,0},{2,3},{3,2},{4,5},{5,4},{6,7},{7,6},{8,9},{9,8},{10,11... | collective-permute-start | bytes 1572872 | tf_op jit(solution)/shard_map/pair_sum/ppermute | solution.py:357
  65.0 1.7 %collective-permute-done.came = bf16[128,2048]{1,0:T(8,128)(2,1)S(1)} collective-permute-done((bf16[128,2048]{1,0:T(8,128)(2,1)}, bf16[128,2048]{1,0:T(8,128)(2,1)S(1)}, u32[]{:S(2)}, u32[]{:S(2)}) %collective-permute-start) | collective-permute-done | bytes 524320 | tf_op jit(solution)/shard_map/pair_sum/ppermute | solution.py:357
  66.7 0.8 copy-done.11
  67.5 2.8 %shard_map.139 = (f32[32,2048]{1,0:T(8,128)}, bf16[32,2048]{1,0:T(8,128)(2,1)}, bf16[32,2048]{1,0:T(8,128)(2,1)}, bf16[32,2048]{1,0:T(8,128)(2,1)}) custom-call(s32[2]{0:T(128)} %pad_add_fusion.at, bf16[256,256]{1,0:T(8,128)(2,1)} %get-tuple-element.38.d_pre, bf16[2048,128]{1,0:T(8,128)(2,1)} %wc.5, bf16[2048,128]{1,0:T(8,128)(2,1)} %wg.5, ...), custom_call_target="tpu_custom_call" | custom-call | flops 1000000000 | bytes 2097152 | tf_op jit(solution)/shard_map/pallas_call | solution.py:37
  70.3 2.2 %collective-permute-start.1 = (bf16[32,2048]{1,0:T(8,128)(2,1)}, bf16[32,2048]{1,0:T(8,128)(2,1)S(1)}, u32[]{:S(2)}, u32[]{:S(2)}) collective-permute-start(bf16[32,2048]{1,0:T(8,128)(2,1)} %get-tuple-element.40), channel_id=1, source_target_pairs={{0,2},{2,4},{4,6},{6,0},{1,3},{3,5},{5,7},{7,1},{8,10},{10,12},{12... | collective-permute-start | bytes 393224 | tf_op jit(solution)/shard_map/sum_x/ppermute | solution.py:31
  72.5 3.7 %collective-permute-start.2 = (bf16[32,2048]{1,0:T(8,128)(2,1)}, bf16[32,2048]{1,0:T(8,128)(2,1)S(1)}, u32[]{:S(2)}, u32[]{:S(2)}) collective-permute-start(bf16[32,2048]{1,0:T(8,128)(2,1)} %get-tuple-element.41), channel_id=1, source_target_pairs={{0,4},{2,6},{4,0},{6,2},{1,5},{3,7},{5,1},{7,3},{8,12},{10,14},{12... | collective-permute-start | bytes 393224 | tf_op jit(solution)/shard_map/sum_x/ppermute | solution.py:31
  76.2 2.7 %collective-permute-start.3 = (bf16[32,2048]{1,0:T(8,128)(2,1)}, bf16[32,2048]{1,0:T(8,128)(2,1)S(1)}, u32[]{:S(2)}, u32[]{:S(2)}) collective-permute-start(bf16[32,2048]{1,0:T(8,128)(2,1)} %get-tuple-element.42), channel_id=1, source_target_pairs={{0,6},{2,0},{4,2},{6,4},{1,7},{3,1},{5,3},{7,5},{8,14},{10,8},{12,... | collective-permute-start | bytes 393224 | tf_op jit(solution)/shard_map/sum_x/ppermute | solution.py:31
  78.9 0.0 collective-permute-done.1.one
  78.9 0.0 copy-start.3
  78.9 1.7 %collective-permute-done.2.two = bf16[32,2048]{1,0:T(8,128)(2,1)S(1)} collective-permute-done((bf16[32,2048]{1,0:T(8,128)(2,1)}, bf16[32,2048]{1,0:T(8,128)(2,1)S(1)}, u32[]{:S(2)}, u32[]{:S(2)}) %collective-permute-start.2) | collective-permute-done | bytes 131104 | tf_op jit(solution)/shard_map/sum_x/ppermute | solution.py:31
  80.6 3.0 %collective-permute-done.3.three = bf16[32,2048]{1,0:T(8,128)(2,1)S(1)} collective-permute-done((bf16[32,2048]{1,0:T(8,128)(2,1)}, bf16[32,2048]{1,0:T(8,128)(2,1)S(1)}, u32[]{:S(2)}, u32[]{:S(2)}) %collective-permute-start.3) | collective-permute-done | bytes 131104 | tf_op jit(solution)/shard_map/sum_x/ppermute | solution.py:31
  83.6 0.0 copy-done.4
  83.6 0.6 copy-done.5
  84.3 1.8 %shard_map.140.own = bf16[32,2048]{1,0:T(8,128)(2,1)} custom-call(f32[32,2048]{1,0:T(8,128)} %get-tuple-element.39.own, bf16[32,2048]{1,0:T(8,128)(2,1)} %copy-done.3, bf16[32,2048]{1,0:T(8,128)(2,1)} %copy-done.4, bf16[32,2048]{1,0:T(8,128)(2,1)} %copy-done.5), custom_call_target="tpu_custom_call" | custom-call | flops 100000000 | bytes 262144 | tf_op jit(solution)/shard_map/pallas_call | solution.py:37
  86.1 4.6 %collective-permute-start.6 = (bf16[32,2048]{1,0:T(8,128)(2,1)}, bf16[32,2048]{1,0:T(8,128)(2,1)S(1)}, u32[]{:S(2)}, u32[]{:S(2)}) collective-permute-start(bf16[32,2048]{1,0:T(8,128)(2,1)} %shard_map.140.own), channel_id=1, source_target_pairs={{0,6},{2,0},{4,2},{6,4},{1,7},{3,1},{5,3},{7,5},{8,14},{10,8},{12,... | collective-permute-start | bytes 393224 | tf_op jit(solution)/shard_map/share_x/ppermute | solution.py:31
  90.6 1.9 %collective-permute-start.5 = (bf16[32,2048]{1,0:T(8,128)(2,1)}, bf16[32,2048]{1,0:T(8,128)(2,1)S(1)}, u32[]{:S(2)}, u32[]{:S(2)}) collective-permute-start(bf16[32,2048]{1,0:T(8,128)(2,1)} %shard_map.140.own), channel_id=1, source_target_pairs={{0,4},{2,6},{4,0},{6,2},{1,5},{3,7},{5,1},{7,3},{8,12},{10,14},{12... | collective-permute-start | bytes 393224 | tf_op jit(solution)/shard_map/share_x/ppermute | solution.py:31
  92.6 2.5 %collective-permute-start.4 = (bf16[32,2048]{1,0:T(8,128)(2,1)}, bf16[32,2048]{1,0:T(8,128)(2,1)S(1)}, u32[]{:S(2)}, u32[]{:S(2)}) collective-permute-start(bf16[32,2048]{1,0:T(8,128)(2,1)} %shard_map.140.own), channel_id=1, source_target_pairs={{0,2},{2,4},{4,6},{6,0},{1,3},{3,5},{5,7},{7,1},{8,10},{10,12},{12... | collective-permute-start | bytes 393224 | tf_op jit(solution)/shard_map/share_x/ppermute | solution.py:31
  95.1 0.0 collective-permute-done.6.three
  95.1 0.0 copy-start.6
  95.1 3.0 %collective-permute-done.5.two = bf16[32,2048]{1,0:T(8,128)(2,1)S(1)} collective-permute-done((bf16[32,2048]{1,0:T(8,128)(2,1)}, bf16[32,2048]{1,0:T(8,128)(2,1)S(1)}, u32[]{:S(2)}, u32[]{:S(2)}) %collective-permute-start.5) | collective-permute-done | bytes 131104 | tf_op jit(solution)/shard_map/share_x/ppermute | solution.py:31
  98.1 3.9 %collective-permute-done.4.one = bf16[32,2048]{1,0:T(8,128)(2,1)S(1)} collective-permute-done((bf16[32,2048]{1,0:T(8,128)(2,1)}, bf16[32,2048]{1,0:T(8,128)(2,1)S(1)}, u32[]{:S(2)}, u32[]{:S(2)}) %collective-permute-start.4) | collective-permute-done | bytes 131104 | tf_op jit(solution)/shard_map/share_x/ppermute | solution.py:31
  102.0 0.7 copy-done.8
  102.7 1.9 %shard_map.141.own = bf16[128,2048]{1,0:T(8,128)(2,1)} custom-call(s32[2]{0:T(128)} %pad_add_fusion.at, bf16[32,2048]{1,0:T(8,128)(2,1)} %shard_map.140.own, bf16[32,2048]{1,0:T(8,128)(2,1)} %copy-done.8, bf16[32,2048]{1,0:T(8,128)(2,1)} %copy-done.7, bf16[32,2048]{1,0:T(8,128)(2,1)} %copy-done.6), custom_call_target="tpu_custom_call" | custom-call | flops 100000000 | bytes 1048576 | tf_op jit(solution)/shard_map/pallas_call | solution.py:37
  104.6 3.1 %collective-permute-start.7 = (bf16[128,2048]{1,0:T(8,128)(2,1)}, bf16[128,2048]{1,0:T(8,128)(2,1)S(1)}, u32[]{:S(2)}, u32[]{:S(2)}) collective-permute-start(bf16[128,2048]{1,0:T(8,128)(2,1)} %shard_map.141.own), channel_id=1, source_target_pairs={{0,1},{1,0},{2,3},{3,2},{4,5},{5,4},{6,7},{7,6},{8,9},{9,8},{10,11... | collective-permute-start | bytes 1572872 | tf_op jit(solution)/shard_map/share_pair/ppermute | solution.py:375
  107.7 0.0 all-to-all-done.2.refs_0_
  107.7 0.0 copy-start.2
  107.7 0.7 copy-done.2
  108.5 1.7 %shard_map.144 = (f32[32,128]{1,0:T(8,128)}, f32[32,128]{1,0:T(8,128)}, f32[4,32,128]{2,1,0:T(8,128)}) custom-call(bf16[16,48,256]{2,1,0:T(8,128)(2,1)} %copy-done.2), custom_call_target="tpu_custom_call" | custom-call | flops 1000000000 | bytes 393216 | tf_op jit(solution)/shard_map/pallas_call | solution.py:37
  110.2 3.3 %all-to-all-start.3 = ((f32[4,32,128]{2,1,0:T(8,128)}), f32[4,32,128]{2,1,0:T(8,128)S(1)}, u32[]{:S(2)}, u32[]{:S(2)}) async-start(f32[4,32,128]{2,1,0:T(8,128)} %get-tuple-element.46), calls=%async_computation.3 | async-start | bytes 131072 | tf_op jit(solution)/shard_map/share_y/all_to_all | solution.py:26
  113.4 0.0 collective-permute-done.7.other
  113.5 0.8 copy-done.1
  114.3 2.2 %shard_map.142 = bf16[256,2048]{1,0:T(8,128)(2,1)} custom-call(s32[2]{0:T(128)} %pad_add_fusion.at, bf16[128,2048]{1,0:T(8,128)(2,1)} %shard_map.141.own, bf16[128,2048]{1,0:T(8,128)(2,1)} %copy-done.1), custom_call_target="tpu_custom_call" | custom-call | flops 100000000 | bytes 2097152 | tf_op jit(solution)/shard_map/pallas_call | solution.py:37
  116.5 1.4 %all-to-all-done.3.small = f32[4,32,128]{2,1,0:T(8,128)S(1)} async-done(((f32[4,32,128]{2,1,0:T(8,128)}), f32[4,32,128]{2,1,0:T(8,128)S(1)}, u32[]{:S(2)}, u32[]{:S(2)}) %all-to-all-start.3) | async-done | bytes 65568 | tf_op jit(solution)/shard_map/share_y/all_to_all | solution.py:26
  117.9 0.6 copy-done.9
  118.5 1.5 %shard_map.145 = (f32[1,128,128]{2,1,0:T(8,128)}, f32[1,128]{1,0:T(1,128)}, f32[1,128]{1,0:T(1,128)}, f32[1,128]{1,0:T(1,128)}) custom-call(f32[4,32,128]{2,1,0:T(8,128)} %copy-done.9), custom_call_target="tpu_custom_call" | custom-call | flops 100000000 | bytes 65536 | tf_op jit(solution)/shard_map/pallas_call | solution.py:37
  (12 shorter events, 0.0 us)
Async XLA Ops:
  5.8 14.8 %all-to-all-start = ((f32[8,8,128]{2,1,0:T(8,128)}), f32[8,8,128]{2,1,0:T(8,128)S(1)}, u32[]{:S(2)}, u32[]{:S(2)}) async-start(f32[8,8,128]{2,1,0:T(8,128)} %get-tuple-element.29), calls=%async_computation | async-start | bytes 65536 | tf_op jit(solution)/shard_map/all_to_all | solution.py:26
  20.6 0.6 copy-start.10
  25.1 18.7 %all-to-all-start.1 = ((bf16[4,544,256]{2,1,0:T(8,128)(2,1)}), bf16[4,544,256]{2,1,0:T(8,128)(2,1)S(1)}, u32[]{:S(2)}, u32[]{:S(2)}) async-start(bf16[4,544,256]{2,1,0:T(8,128)(2,1)} %get-tuple-element.43), calls=%async_computation.1 | async-start | bytes 2228224 | tf_op jit(solution)/shard_map/sum_y/all_to_all | solution.py:26
  43.7 1.0 copy-start
  46.8 60.9 %all-to-all-start.2 = ((bf16[16,48,256]{2,1,0:T(8,128)(2,1)}), bf16[16,48,256]{2,1,0:T(8,128)(2,1)S(1)}, u32[]{:S(2)}, u32[]{:S(2)}) async-start(bf16[16,48,256]{2,1,0:T(8,128)(2,1)} %shard_map.143), calls=%async_computation.2 | async-start | bytes 786432 | tf_op jit(solution)/shard_map/sum_z/all_to_all | solution.py:26
  60.9 5.8 %collective-permute-start = (bf16[128,2048]{1,0:T(8,128)(2,1)}, bf16[128,2048]{1,0:T(8,128)(2,1)S(1)}, u32[]{:S(2)}, u32[]{:S(2)}) collective-permute-start(bf16[128,2048]{1,0:T(8,128)(2,1)} %shard_map.138), channel_id=1, source_target_pairs={{0,1},{1,0},{2,3},{3,2},{4,5},{5,4},{6,7},{7,6},{8,9},{9,8},{10,11... | collective-permute-start | bytes 1572872 | tf_op jit(solution)/shard_map/pair_sum/ppermute | solution.py:357
  66.7 0.8 copy-start.11
  70.3 8.6 %collective-permute-start.1 = (bf16[32,2048]{1,0:T(8,128)(2,1)}, bf16[32,2048]{1,0:T(8,128)(2,1)S(1)}, u32[]{:S(2)}, u32[]{:S(2)}) collective-permute-start(bf16[32,2048]{1,0:T(8,128)(2,1)} %get-tuple-element.40), channel_id=1, source_target_pairs={{0,2},{2,4},{4,6},{6,0},{1,3},{3,5},{5,7},{7,1},{8,10},{10,12},{12... | collective-permute-start | bytes 393224 | tf_op jit(solution)/shard_map/sum_x/ppermute | solution.py:31
  72.5 8.1 %collective-permute-start.2 = (bf16[32,2048]{1,0:T(8,128)(2,1)}, bf16[32,2048]{1,0:T(8,128)(2,1)S(1)}, u32[]{:S(2)}, u32[]{:S(2)}) collective-permute-start(bf16[32,2048]{1,0:T(8,128)(2,1)} %get-tuple-element.41), channel_id=1, source_target_pairs={{0,4},{2,6},{4,0},{6,2},{1,5},{3,7},{5,1},{7,3},{8,12},{10,14},{12... | collective-permute-start | bytes 393224 | tf_op jit(solution)/shard_map/sum_x/ppermute | solution.py:31
  76.2 7.4 %collective-permute-start.3 = (bf16[32,2048]{1,0:T(8,128)(2,1)}, bf16[32,2048]{1,0:T(8,128)(2,1)S(1)}, u32[]{:S(2)}, u32[]{:S(2)}) collective-permute-start(bf16[32,2048]{1,0:T(8,128)(2,1)} %get-tuple-element.42), channel_id=1, source_target_pairs={{0,6},{2,0},{4,2},{6,4},{1,7},{3,1},{5,3},{7,5},{8,14},{10,8},{12,... | collective-permute-start | bytes 393224 | tf_op jit(solution)/shard_map/sum_x/ppermute | solution.py:31
  78.9 4.7 %copy-start.3 = (bf16[32,2048]{1,0:T(8,128)(2,1)}, bf16[32,2048]{1,0:T(8,128)(2,1)S(1)}, u32[]{:S(2)}) copy-start(bf16[32,2048]{1,0:T(8,128)(2,1)S(1)} %collective-permute-done.1.one) | copy-start | bytes 393220
  80.6 3.1 %copy-start.4 = (bf16[32,2048]{1,0:T(8,128)(2,1)}, bf16[32,2048]{1,0:T(8,128)(2,1)S(1)}, u32[]{:S(2)}) copy-start(bf16[32,2048]{1,0:T(8,128)(2,1)S(1)} %collective-permute-done.2.two) | copy-start | bytes 393220
  83.6 0.7 copy-start.5
  86.1 9.0 %collective-permute-start.6 = (bf16[32,2048]{1,0:T(8,128)(2,1)}, bf16[32,2048]{1,0:T(8,128)(2,1)S(1)}, u32[]{:S(2)}, u32[]{:S(2)}) collective-permute-start(bf16[32,2048]{1,0:T(8,128)(2,1)} %shard_map.140.own), channel_id=1, source_target_pairs={{0,6},{2,0},{4,2},{6,4},{1,7},{3,1},{5,3},{7,5},{8,14},{10,8},{12,... | collective-permute-start | bytes 393224 | tf_op jit(solution)/shard_map/share_x/ppermute | solution.py:31
  90.6 7.4 %collective-permute-start.5 = (bf16[32,2048]{1,0:T(8,128)(2,1)}, bf16[32,2048]{1,0:T(8,128)(2,1)S(1)}, u32[]{:S(2)}, u32[]{:S(2)}) collective-permute-start(bf16[32,2048]{1,0:T(8,128)(2,1)} %shard_map.140.own), channel_id=1, source_target_pairs={{0,4},{2,6},{4,0},{6,2},{1,5},{3,7},{5,1},{7,3},{8,12},{10,14},{12... | collective-permute-start | bytes 393224 | tf_op jit(solution)/shard_map/share_x/ppermute | solution.py:31
  92.6 9.4 %collective-permute-start.4 = (bf16[32,2048]{1,0:T(8,128)(2,1)}, bf16[32,2048]{1,0:T(8,128)(2,1)S(1)}, u32[]{:S(2)}, u32[]{:S(2)}) collective-permute-start(bf16[32,2048]{1,0:T(8,128)(2,1)} %shard_map.140.own), channel_id=1, source_target_pairs={{0,2},{2,4},{4,6},{6,0},{1,3},{3,5},{5,7},{7,1},{8,10},{10,12},{12... | collective-permute-start | bytes 393224 | tf_op jit(solution)/shard_map/share_x/ppermute | solution.py:31
  95.1 6.9 %copy-start.6 = (bf16[32,2048]{1,0:T(8,128)(2,1)}, bf16[32,2048]{1,0:T(8,128)(2,1)S(1)}, u32[]{:S(2)}) copy-start(bf16[32,2048]{1,0:T(8,128)(2,1)S(1)} %collective-permute-done.6.three) | copy-start | bytes 393220
  98.1 3.9 %copy-start.7 = (bf16[32,2048]{1,0:T(8,128)(2,1)}, bf16[32,2048]{1,0:T(8,128)(2,1)S(1)}, u32[]{:S(2)}) copy-start(bf16[32,2048]{1,0:T(8,128)(2,1)S(1)} %collective-permute-done.5.two) | copy-start | bytes 393220
  102.0 0.7 copy-start.8
  104.6 8.9 %collective-permute-start.7 = (bf16[128,2048]{1,0:T(8,128)(2,1)}, bf16[128,2048]{1,0:T(8,128)(2,1)S(1)}, u32[]{:S(2)}, u32[]{:S(2)}) collective-permute-start(bf16[128,2048]{1,0:T(8,128)(2,1)} %shard_map.141.own), channel_id=1, source_target_pairs={{0,1},{1,0},{2,3},{3,2},{4,5},{5,4},{6,7},{7,6},{8,9},{9,8},{10,11... | collective-permute-start | bytes 1572872 | tf_op jit(solution)/shard_map/share_pair/ppermute | solution.py:375
  107.7 0.7 copy-start.2
  110.2 7.7 %all-to-all-start.3 = ((f32[4,32,128]{2,1,0:T(8,128)}), f32[4,32,128]{2,1,0:T(8,128)S(1)}, u32[]{:S(2)}, u32[]{:S(2)}) async-start(f32[4,32,128]{2,1,0:T(8,128)} %get-tuple-element.46), calls=%async_computation.3 | async-start | bytes 131072 | tf_op jit(solution)/shard_map/share_y/all_to_all | solution.py:26
  113.5 0.8 copy-start.1
  117.9 0.6 copy-start.9
